TPU v7x, 32 devices: a whole 2x2x4 slice. The times are simulated.
32 devices in a mesh: sp: 8 (over z, x), tp: 4 (over y, core).
Axes of the slice: x: 2, y: 2, z: 4, core: 2. Of those that a mesh axis runs over, the one named last changes fastest.
Arguments:
- queries: bfloat16 [1536, 1536], P('sp', 'tp'), may hold values from -64 to 64
- latents: bfloat16 [1536, 512], P('sp'), may hold values from -6 to 6
- rope_key: bfloat16 [1536, 32], P('sp'), may hold values from -64 to 64
- w_key: bfloat16 [512, 1024], P(None, 'tp'), may hold values from -0.25 to 0.25
- w_value: bfloat16 [512, 1024], P(None, 'tp'), may hold values from -0.25 to 0.25
- w_out: bfloat16 [1024, 2048], P('tp'), may hold values from -0.59765625 to 0.59765625
- resid: bfloat16 [1536, 2048], P('sp', 'tp'), may hold values from -12 to 12
- gain_mix: float32 [2048], P('tp'), may hold values from 0.1 to 1.9
- w_gate: bfloat16 [2048, 3072], P('sp', 'tp'), may hold values from -0.125 to 0.125
- w_up: bfloat16 [2048, 3072], P('sp', 'tp'), may hold values from -0.125 to 0.125
- w_down: bfloat16 [3072, 2048], P('tp', 'sp'), may hold values from -0.41992188 to 0.41992188
- gain_out: float32 [2048], P('tp'), may hold values from 0.1 to 1.9
Outputs:
- layer_out: bfloat16 [1536, 2048], P('sp', 'tp')
All inputs are finite; a program needn't handle non-finite values.
Results may differ from a plain program's by a relative error of at most 0.014.
Values may be sent and summed in bfloat16 or wider, within the bound.
A program may use at most 128 MiB of HBM per device.

v0:
```python
import jax
import jax.numpy as jnp
from jax import lax
from jax.sharding import PartitionSpec as P

NOPE = 64
ROPE = 32
VDIM = 64
GRID_W = 64


ROTARY_BASE = 10000.0
NORM_EPSILON = 1e-06
DEEP_ALPHA = 8.0**0.25
HALF_STEP = 0.5


def rotary_tables(positions, rotary_width, grid_width):
    grid_rows = (positions // grid_width).astype(jnp.float32)
    grid_cols = (positions % grid_width).astype(jnp.float32)
    freq_count = rotary_width // 4
    inverse = ROTARY_BASE ** (-jnp.arange(freq_count, dtype=jnp.float32) / freq_count)
    angle_table = jnp.concatenate(
        [grid_rows[:, None] * inverse, grid_cols[:, None] * inverse], axis=-1
    )
    return (jnp.cos(angle_table), jnp.sin(angle_table))


def rotate(vectors, cosine, sine):
    half_width = vectors.shape[-1] // 2
    leading = vectors[..., :half_width].astype(jnp.float32)
    trailing = vectors[..., half_width:].astype(jnp.float32)
    return jnp.concatenate(
        [leading * cosine - trailing * sine, leading * sine + trailing * cosine], axis=-1
    ).astype(jnp.bfloat16)


def attend_block(state, key_block, query_pair):
    maxima, totals, running = state
    key_nope, value_rows, key_rope = key_block
    q_nope, q_rope = query_pair
    head_count = q_nope.shape[1]
    rows_here = key_nope.shape[0]
    key_nope = key_nope.reshape(rows_here, head_count, -1)
    value_rows = value_rows.reshape(rows_here, head_count, -1)
    score_scale = (q_nope.shape[2] + q_rope.shape[2]) ** (-0.5)
    scores = jnp.einsum("qhd,khd->hqk", q_nope, key_nope, preferred_element_type=jnp.float32)
    scores = (
        scores + jnp.einsum("qhd,kd->hqk", q_rope, key_rope, preferred_element_type=jnp.float32)
    ) * score_scale
    new_max = jnp.maximum(maxima, jnp.max(scores, axis=-1))
    weights = jnp.exp(scores - new_max[:, :, None])
    factor = jnp.exp(maxima - new_max)
    totals = totals * factor + jnp.sum(weights, axis=-1)
    update = jnp.einsum(
        "hqk,khd->qhd", weights.astype(jnp.bfloat16), value_rows, preferred_element_type=jnp.float32
    )
    running = running * jnp.transpose(factor)[:, :, None] + update
    return (new_max, totals, running)


def block_length(length):
    block_rows = length
    while block_rows > 2048 and block_rows % 2 == 0:
        block_rows = block_rows // 2
    return block_rows


def fold_keys(state, pieces, query_pair):
    length = pieces[0].shape[0]
    block_rows = block_length(length)
    if block_rows == length:
        return attend_block(state, pieces, query_pair)
    stacked = tuple(
        (member.reshape(length // block_rows, block_rows, member.shape[1]) for member in pieces)
    )

    def one_block(partial_value, key_block):
        return (attend_block(partial_value, key_block, query_pair), None)

    state, unused = lax.scan(one_block, state, stacked)
    return state


def split_norm(rows_in, gain_row):
    width_total = rows_in.shape[1] * lax.axis_size("tp")
    row_sums, squares = lax.psum(
        (jnp.sum(rows_in, axis=1), jnp.sum(rows_in * rows_in, axis=1)), "tp"
    )
    row_mean = row_sums / width_total
    variance = squares / width_total - row_mean * row_mean
    return (
        (rows_in - row_mean[:, None]) * lax.rsqrt(variance + NORM_EPSILON)[:, None] * gain_row
    ).astype(jnp.bfloat16)


def local(
    queries,
    latents,
    rope_key,
    w_key,
    w_value,
    w_out,
    resid,
    gain_mix,
    w_gate,
    w_up,
    w_down,
    gain_out,
):
    local_rows = queries.shape[0]
    head_count = w_key.shape[1] // NOPE
    offset = lax.axis_index("sp") * local_rows
    positions = offset + jnp.arange(local_rows, dtype=jnp.int32)
    cosine, sine = rotary_tables(positions, ROPE, GRID_W)
    key_rot = rotate(rope_key, cosine, sine)
    shaped = queries.reshape(local_rows, head_count, NOPE + ROPE)
    q_nope = shaped[:, :, :NOPE]
    q_rot = rotate(shaped[:, :, NOPE:], cosine[:, None, :], sine[:, None, :])
    query_pair = (q_nope, q_rot)
    start_state = (
        jnp.full((head_count, local_rows), -jnp.inf, jnp.float32),
        jnp.zeros((head_count, local_rows), jnp.float32),
        jnp.zeros((local_rows, head_count, VDIM), jnp.float32),
    )
    quarter = local_rows // lax.axis_size("tp")
    first_row = lax.axis_index("tp") * quarter
    latent_part = lax.dynamic_slice_in_dim(latents, first_row, quarter, 0)
    rotary_part = lax.dynamic_slice_in_dim(key_rot, first_row, quarter, 0)
    latent_all, rotary_all = (
        lax.all_gather(latent_part, "sp", axis=0, tiled=True),
        lax.all_gather(rotary_part, "sp", axis=0, tiled=True),
    )
    pieces = (
        lax.all_gather(latent_all, "tp", axis=0, tiled=True),
        lax.all_gather(rotary_all, "tp", axis=0, tiled=True),
    )
    key_nope = jnp.dot(pieces[0], w_key, preferred_element_type=jnp.float32).astype(jnp.bfloat16)
    value_rows = jnp.dot(pieces[0], w_value, preferred_element_type=jnp.float32).astype(
        jnp.bfloat16
    )
    state = fold_keys(start_state, (key_nope, value_rows, pieces[1]), query_pair)
    maxima, totals, running = state
    heads_out = (
        (running / jnp.transpose(totals)[:, :, None])
        .reshape(local_rows, head_count * VDIM)
        .astype(jnp.bfloat16)
    )
    projected = jnp.dot(heads_out, w_out, preferred_element_type=jnp.float32)
    attn_cols = lax.psum_scatter(
        projected.astype(jnp.bfloat16), "tp", scatter_dimension=1, tiled=True
    ).astype(jnp.float32)
    hidden_in = split_norm(DEEP_ALPHA * resid.astype(jnp.float32) + attn_cols, gain_mix)
    whole_rows = lax.all_gather(hidden_in, "tp", axis=1, tiled=True)
    pieces = (
        lax.all_gather(w_gate, "sp", axis=0, tiled=True),
        lax.all_gather(w_up, "sp", axis=0, tiled=True),
    )
    gate_sum = jnp.dot(whole_rows, pieces[0], preferred_element_type=jnp.float32)
    up_sum = jnp.dot(whole_rows, pieces[1], preferred_element_type=jnp.float32)
    hidden = (jax.nn.silu(gate_sum) * up_sum).astype(jnp.bfloat16)
    down_terms = jnp.dot(
        hidden, lax.all_gather(w_down, "sp", axis=1, tiled=True), preferred_element_type=jnp.float32
    )
    mixer_cols = lax.psum_scatter(
        down_terms.astype(jnp.bfloat16), "tp", scatter_dimension=1, tiled=True
    ).astype(jnp.float32)
    return split_norm(DEEP_ALPHA * hidden_in.astype(jnp.float32) + HALF_STEP * mixer_cols, gain_out)


def solution(mesh):
    placed = (
        P("sp", "tp"),
        P("sp", None),
        P("sp", None),
        P(None, "tp"),
        P(None, "tp"),
        P("tp", None),
        P("sp", "tp"),
        P("tp"),
        P("sp", "tp"),
        P("sp", "tp"),
        P("tp", "sp"),
        P("tp"),
    )
    return jax.shard_map(
        local, mesh=mesh, in_specs=placed, out_specs=P("sp", "tp"), check_vma=False
    )
```

profile of v0, /device:TPU:0, one launch (start us, length us, event | category | flops | bytes accessed | tf_op | source)
XLA Modules:
  0.0 324.2 jit_solution(2186468816205035295)
XLA Ops:
  7.4 0.0 all-gather.6.cloned.1.call-start
  7.4 0.9 constant_dynamic-slice_fusion
  8.3 34.8 %all_gather.24 = bf16[384,512]{1,0:T(8,128)(2,1)} all-gather(bf16[48,512]{1,0:T(8,128)(2,1)S(1)} %constant_dynamic-slice_fusion), channel_id=1, replica_groups=mesh['sp'=8,'tp'=4] {'sp'}, dimensions={0}, use_global_device_ids=true | all-gather | bytes 442368 | tf_op jit(solution)/shard_map/all_gather | solution.py:131
  43.1 0.0 all-gather.6.cloned.1.call-update
  43.1 0.0 reduce-scatter.3.cloned.1.call-start
  43.2 0.1 broadcast_multiply_fusion.1
  43.3 0.8 fusion.40
  44.1 0.1 fusion.44
  44.2 30.5 %all-gather = bf16[8,48,32]{1,2,0:T(8,128)(2,1)S(1)} all-gather(bf16[1,48,32]{1,2,0:T(8,128)(2,1)S(1)} %fusion.44), channel_id=1, replica_groups=mesh['sp'=8,'tp'=4] {'sp'}, dimensions={0}, use_global_device_ids=true | all-gather | bytes 27648 | tf_op jit(solution)/shard_map/all_gather | solution.py:132
  74.7 0.1 reshape.118
  74.9 1.0 copy.16
  75.9 5.3 %all_gather.27 = bf16[1536,32]{0,1:T(8,128)(2,1)S(1)} all-gather(bf16[384,32]{0,1:T(8,128)(2,1)S(1)} %reshape.118), channel_id=1, replica_groups=mesh['sp'=8,'tp'=4] {'tp'}, dimensions={0}, use_global_device_ids=true | all-gather | bytes 122880 | tf_op jit(solution)/shard_map/all_gather | solution.py:136
  81.3 2.9 fusion.28
  84.2 2.0 convolution_convert_fusion.1
  86.2 3.3 %fusion.50 = (f32[4,192]{1,0:T(4,128)S(1)}, f32[4,192,1536]{2,1,0:T(8,128)S(1)}) fusion(f32[1536,192,4]{0,1,2:T(8,128)} %fusion.28, bf16[1536,4,64]{0,2,1:T(8,128)(2,1)S(1)} %bitcast.45, bf16[192,4,96]{0,2,1:T(8,128)(2,1)S(1)} %bitcast.47), kind=kOutput, calls=%fused_computation.82 | convolution fusion | flops 154533120 | bytes 10357760 | tf_op jit(solution)/shard_map/qhd,khd->hqk/dot_general | solution.py:47
  89.5 0.0 copy-start.1
  89.5 0.0 copy-start.4
  89.6 0.8 fusion.1
  90.3 0.6 copy-done.1
  90.9 0.0 copy-done.4
  90.9 0.6 convolution_convert_fusion
  91.6 1.0 fusion.16
  92.6 0.0 copy-start.5
  92.6 1.3 convolution_convert_fusion.3
  93.9 0.0 reduce-scatter.3.cloned.1.call-update
  93.9 0.0 all-gather.8.cloned.1.call-start
  94.0 0.5 all-gather.8.cloned.1.call-update
  94.5 0.0 all-gather.10.cloned.1.call-start
  94.6 0.5 all-gather.10.cloned.1.call-update
  95.1 0.0 all-gather.12.cloned.1.call-start
  95.1 0.5 all-gather.12.cloned.1.call-update
  95.7 0.0 reduce-scatter.5.cloned.1.call-start
  95.7 22.5 %reduce-scatter.3.cloned.1.call-done = bf16[192,512]{1,0:T(8,128)(2,1)} async-done(((bf16[192,2048]{1,0:T(8,128)(2,1)}), bf16[192,512]{1,0:T(8,128)(2,1)}) %reduce-scatter.3.cloned.1.call-update) | async-done | bytes 196624 | tf_op jit(solution)/shard_map/reduce_scatter | solution.py:150
  118.3 1.1 fusion.24
  119.4 5.8 %all-reduce.1 = (f32[192]{0:T(256)S(1)}, f32[192]{0:T(256)S(1)}) all-reduce(f32[192]{0:T(256)S(1)} %get-tuple-element.8, f32[192]{0:T(256)S(1)} %get-tuple-element.7), channel_id=1, replica_groups=mesh['sp'=8,'tp'=4] {'tp'}, use_global_device_ids=true, to_apply=%region_6.7 | all-reduce | flops 384 | bytes 3072 | tf_op jit(solution)/shard_map/psum | solution.py:87
  125.2 1.1 multiply_convert_fusion.1
  126.2 8.3 %all_gather.28 = bf16[192,2048]{1,0:T(8,128)(2,1)S(1)} all-gather(bf16[192,512]{1,0:T(8,128)(2,1)S(1)} %multiply_convert_fusion.1), channel_id=1, replica_groups=mesh['sp'=8,'tp'=4] {'tp'}, dimensions={1}, use_global_device_ids=true | all-gather | bytes 983040 | tf_op jit(solution)/shard_map/all_gather | solution.py:154
  134.5 22.9 %all-gather.8.cloned.1.call-done = bf16[2048,768]{1,0:T(8,128)(2,1)} async-done(((bf16[256,768]{1,0:T(8,128)(2,1)}), bf16[2048,768]{1,0:T(8,128)(2,1)}) %all-gather.8.cloned.1.call-update) | async-done | bytes 3145744 | tf_op jit(solution)/shard_map/all_gather | solution.py:156
  157.5 2.7 fusion.51
  160.2 0.0 copy-start.6
  160.2 58.0 %all-gather.10.cloned.1.call-done = bf16[2048,768]{1,0:T(8,128)(2,1)} async-done(((bf16[256,768]{1,0:T(8,128)(2,1)}), bf16[2048,768]{1,0:T(8,128)(2,1)}) %all-gather.10.cloned.1.call-update) | async-done | bytes 3145744 | tf_op jit(solution)/shard_map/all_gather | solution.py:157
  218.1 63.1 %all-gather.12.cloned.1.call-done = bf16[768,2048]{1,0:T(8,128)(2,1)} async-done(((bf16[768,256]{1,0:T(8,128)(2,1)}), bf16[768,2048]{1,0:T(8,128)(2,1)}) %all-gather.12.cloned.1.call-update) | async-done | bytes 3145744 | tf_op jit(solution)/shard_map/all_gather | solution.py:163
  281.2 5.4 %convolution_convert_fusion.2 = bf16[192,2048]{1,0:T(8,128)(2,1)} fusion(bf16[768,2048]{1,0:T(8,128)(2,1)} %all-gather.12.cloned.1.call-done, bf16[192,2048]{1,0:T(8,128)(2,1)S(1)} %all_gather.28, bf16[2048,768]{1,0:T(8,128)(2,1)} %all-gather.10.cloned.1.call-done, f32[192,768]{1,0:T(8,128)S(1)} %fusion.51), kind=kOutput, calls=%fused_computation.7 | convolution fusion | flops 1209237504 | bytes 8454144 | tf_op jit(solution)/shard_map/dot_general | solution.py:162
  286.6 0.0 reduce-scatter.5.cloned.1.call-update
  286.6 21.6 %reduce-scatter.5.cloned.1.call-done = bf16[192,512]{1,0:T(8,128)(2,1)} async-done(((bf16[192,2048]{1,0:T(8,128)(2,1)}), bf16[192,512]{1,0:T(8,128)(2,1)}) %reduce-scatter.5.cloned.1.call-update) | async-done | bytes 196624 | tf_op jit(solution)/shard_map/reduce_scatter | solution.py:165
  308.2 1.1 fusion.26
  309.3 5.8 %all-reduce = (f32[192]{0:T(256)S(1)}, f32[192]{0:T(256)S(1)}) all-reduce(f32[192]{0:T(256)S(1)} %get-tuple-element.6, f32[192]{0:T(256)S(1)} %get-tuple-element.5), channel_id=1, replica_groups=mesh['sp'=8,'tp'=4] {'tp'}, use_global_device_ids=true, to_apply=%region_11.12 | all-reduce | flops 384 | bytes 3072 | tf_op jit(solution)/shard_map/psum | solution.py:87
  315.1 1.7 multiply_convert_fusion
  (17 shorter events, 0.1 us)
Async XLA Ops:
  7.4 85.2 %copy-start = (bf16[256,2048]{1,0:T(8,128)(2,1)S(1)}, bf16[256,2048]{1,0:T(8,128)(2,1)}, u32[]{:S(2)}) copy-start(bf16[256,2048]{1,0:T(8,128)(2,1)} %param.17) | copy-start | bytes 3145732
  7.4 76.8 %all-gather.6.cloned.1.call-start = ((), (), s32[]{:S(2)}) async-start(), calls=%async_computation.2 | async-start | bytes 1966080 | tf_op jit(solution)/shard_map/all_gather | solution.py:135
  43.1 41.1 %copy-start.3 = (bf16[512,256]{1,0:T(8,128)(2,1)S(1)}, bf16[512,256]{1,0:T(8,128)(2,1)}, u32[]{:S(2)}) copy-start(bf16[512,256]{1,0:T(8,128)(2,1)} %param.15) | copy-start | bytes 786436
  43.1 75.1 %reduce-scatter.3.cloned.1.call-start = ((), (), s32[]{:S(2)}) async-start(), calls=%async_computation.3 | async-start | bytes 983040 | tf_op jit(solution)/shard_map/reduce_scatter | solution.py:150
  89.5 1.4 copy-start.1
  89.5 1.4 copy-start.4
  92.6 25.7 %copy-start.2 = (bf16[192,512]{1,0:T(8,128)(2,1)S(1)}, bf16[192,512]{1,0:T(8,128)(2,1)}, u32[]{:S(2)}) copy-start(bf16[192,512]{1,0:T(8,128)(2,1)} %param.18) | copy-start | bytes 589828
  92.6 32.6 %copy-start.5 = (f32[512]{0:T(512)S(1)}, f32[512]{0:T(512)}, u32[]{:S(2)}) copy-start(f32[512]{0:T(512)} %param.19) | copy-start | bytes 6148
  93.9 63.6 %all-gather.8.cloned.1.call-start = ((), (), s32[]{:S(2)}) async-start(), calls=%async_computation.4 | async-start | bytes 3538944 | tf_op jit(solution)/shard_map/all_gather | solution.py:156
  94.5 123.6 %all-gather.10.cloned.1.call-start = ((), (), s32[]{:S(2)}) async-start(), calls=%async_computation.5 | async-start | bytes 3538944 | tf_op jit(solution)/shard_map/all_gather | solution.py:157
  95.1 186.1 %all-gather.12.cloned.1.call-start = ((), (), s32[]{:S(2)}) async-start(), calls=%async_computation.6 | async-start | bytes 3538944 | tf_op jit(solution)/shard_map/all_gather | solution.py:163
  95.7 212.5 %reduce-scatter.5.cloned.1.call-start = ((), (), s32[]{:S(2)}) async-start(), calls=%async_computation.7 | async-start | bytes 983040 | tf_op jit(solution)/shard_map/reduce_scatter | solution.py:165
  160.2 154.9 %copy-start.6 = (f32[512]{0:T(512)S(1)}, f32[512]{0:T(512)}, u32[]{:S(2)}) copy-start(f32[512]{0:T(512)} %param.23) | copy-start | bytes 6148
Sparse Core Ops, SparseCore 0:
  43.3 20.5 all-gather.5
  94.0 24.1 reduce-scatter.2
  286.8 21.3 reduce-scatter.4
Sparse Core Ops, SparseCore 1:
  96.6 60.8 all-gather.7
  159.5 58.5 all-gather.9
  220.1 61.1 all-gather.11
where the time goes:
time: 325 us; the launch traced here: 324 us
  waiting for transfers between devices  190 us (58%)
  blocking collectives  90.5 us (28%)
  matrix products  19.2 us (6%)
  between operations  14.9 us (5%)
  other arithmetic  6.87 us (2%)
    all_gather x1, waiting for transfers between devices, local(): lax.all_gather(w_down, 'sp', axis=1, tiled=True)  63.1 us
    all_gather x1, waiting for transfers between devices, local(): lax.all_gather(w_up, 'sp', axis=0, tiled=True)  58 us
    all_gather x1, blocking collectives, local(): lax.all_gather(latent_part, 'sp', axis=0, tiled=True)  34.8 us
    all_gather x1, blocking collectives, local(): lax.all_gather(rotary_part, 'sp', axis=0, tiled=True)  30.5 us
    all_gather x1, waiting for transfers between devices, local(): lax.all_gather(w_gate, 'sp', axis=0, tiled=True)  22.9 us
    reduce_scatter x1, waiting for transfers between devices, local(): lax.psum_scatter(projected.astype(jnp.bfloat16), 'tp', scatter_dimension=...  22.5 us
    reduce_scatter x1, waiting for transfers between devices, local(): lax.psum_scatter(down_terms.astype(jnp.bfloat16), 'tp', scatter_dimension...  21.6 us
    psum x2, blocking collectives, split_norm(): lax.psum((jnp.sum(rows_in, axis=1), jnp.sum(rows_in * rows_in, axis=1)),...  11.5 us
  transfers between devices with their start and end apart: 6, of which 5 were waited for; matrix products, arithmetic and copies ran while one was open for 3% of the time, Pallas kernels for 0%

commit v1 on v0

v1 whole, which is shorter than its diff:
```python
import functools

import jax
import jax.numpy as jnp
from jax import lax
from jax.experimental import pallas as pl
from jax.experimental.pallas import tpu as pltpu
from jax.sharding import PartitionSpec as P

NOPE = 64
ROPE = 32
VDIM = 64
GRID_W = 64
LANES = 128

ROTARY_BASE = 10000.0
NORM_EPSILON = 1e-06
DEEP_ALPHA = 8.0**0.25
HALF_STEP = 0.5
MESH = pl.DeviceIdType.MESH


def rotary_tables(positions, rotary_width, grid_width):
    grid_rows = (positions // grid_width).astype(jnp.float32)
    grid_cols = (positions % grid_width).astype(jnp.float32)
    freq_count = rotary_width // 4
    inverse = ROTARY_BASE ** (-jnp.arange(freq_count, dtype=jnp.float32) / freq_count)
    angle_table = jnp.concatenate(
        [grid_rows[:, None] * inverse, grid_cols[:, None] * inverse], axis=-1
    )
    return (jnp.cos(angle_table), jnp.sin(angle_table))


def rotate(vectors, cosine, sine):
    half_width = vectors.shape[-1] // 2
    leading = vectors[..., :half_width].astype(jnp.float32)
    trailing = vectors[..., half_width:].astype(jnp.float32)
    return jnp.concatenate(
        [leading * cosine - trailing * sine, leading * sine + trailing * cosine], axis=-1
    ).astype(jnp.bfloat16)


def ring_device(place, count):
    return jnp.where(place < count // 2, 2 * place, 2 * (count - 1 - place) + 1)


def ring_place(index, count):
    return jnp.where(index % 2 == 0, index // 2, count - 1 - index // 2)


def dot(left, right):
    return jnp.dot(left, right, preferred_element_type=jnp.float32)


def dot_nt(left, right):
    return lax.dot_general(
        left, right, (((1,), (1,)), ((), ())), preferred_element_type=jnp.float32
    )


def layer_kernel(
    n_sp,
    n_tp,
    splits,
    q_ref,
    lat_ref,
    wk_ref,
    wv_ref,
    wo_ref,
    resid_ref,
    gain_mix_ref,
    gain_out_ref,
    wg_ref,
    wu_ref,
    wd_ref,
    out_ref,
    lat_all,
    keys,
    values,
    gate_all,
    up_all,
    down_all,
    heads,
    part_send,
    part_recv,
    stat_send,
    stat_recv,
    rows_all,
    part2_send,
    part2_recv,
    stat2_send,
    stat2_recv,
    local_sem,
    lat_send,
    lat_recv,
    share_send,
    share_recv,
    ring_send,
    ring_recv,
    tp_send,
    tp_recv,
):
    sp = lax.axis_index("sp")
    tp = lax.axis_index("tp")
    place = ring_place(sp, n_sp)
    ahead = ring_device((place + 1) % n_sp, n_sp)
    behind = ring_device((place + n_sp - 1) % n_sp, n_sp)
    targets = (ahead, behind)
    partner = tp + 1 - 2 * (tp % 2)
    core = tp % 2
    n_rows = q_ref.shape[1]
    head_count = q_ref.shape[0]
    lat_rows = lat_all.shape[2]
    n_cols = out_ref.shape[1]

    own = []
    lat_own = pltpu.make_async_copy(lat_ref, lat_all.at[sp], local_sem.at[0])
    lat_own.start()
    weights = (gate_all, up_all, down_all)
    for i, (source, target) in enumerate(
        zip((wg_ref, wu_ref, wd_ref), weights)
    ):
        copy = pltpu.make_async_copy(source, target.at[sp], local_sem.at[i + 1])
        copy.start()
        own.append(copy)

    barrier = pltpu.get_barrier_semaphore()
    for device in targets:
        pl.semaphore_signal(barrier, inc=1, device_id={"sp": device}, device_id_type=MESH)
    for step in range(1, n_tp):
        pl.semaphore_signal(
            barrier, inc=1, device_id={"tp": (tp + step) % n_tp}, device_id_type=MESH
        )
    pl.semaphore_wait(barrier, 2 + n_tp - 1)

    def origin(hop, direction):
        if direction == 0:
            return ring_device((place + n_sp - hop) % n_sp, n_sp)
        return ring_device((place + hop) % n_sp, n_sp)

    def lat_copy(hop, direction):
        block = lat_all.at[origin(hop - 1, direction), core * 2 + direction]
        return pltpu.make_async_remote_copy(
            src_ref=block,
            dst_ref=block,
            send_sem=lat_send.at[direction],
            recv_sem=lat_recv.at[direction, hop - 1],
            device_id={"sp": targets[direction]},
            device_id_type=MESH,
        )

    def lat_arrival(hop, direction):
        block = lat_all.at[origin(hop, direction), core * 2 + direction]
        return pltpu.make_async_remote_copy(
            src_ref=block,
            dst_ref=block,
            send_sem=lat_send.at[direction],
            recv_sem=lat_recv.at[direction, hop - 1],
            device_id={"sp": targets[direction]},
            device_id_type=MESH,
        )

    def share_copy(hop, direction, which):
        block = lat_all.at[origin(hop, direction), which * 2 + direction]
        return pltpu.make_async_remote_copy(
            src_ref=block,
            dst_ref=block,
            send_sem=share_send.at[direction],
            recv_sem=share_recv.at[direction, hop - 1],
            device_id={"tp": partner},
            device_id_type=MESH,
        )

    piece_rows = wg_ref.shape[0] // (2 * splits)

    def ring_copy(array, piece, hop, direction, arriving):
        block = origin(hop if arriving else hop - 1, direction)
        rows = pl.ds((direction * splits + piece) * piece_rows, piece_rows)
        ref = weights[array].at[block, rows]
        return pltpu.make_async_remote_copy(
            src_ref=ref,
            dst_ref=ref,
            send_sem=ring_send.at[array, piece, direction],
            recv_sem=ring_recv.at[array, piece, direction, hop - 1],
            device_id={"sp": targets[direction]},
            device_id_type=MESH,
        )

    started = set()

    def ring_step(array, piece, hop):
        if hop == 1 and array not in started:
            own[array].wait()
            started.add(array)
        for direction in range(2):
            if hop > 1:
                ring_copy(array, piece, hop - 1, direction, True).wait_recv()
                ring_copy(array, piece, hop - 1, direction, False).wait_send()
            if hop < n_sp:
                ring_copy(array, piece, hop, direction, False).start()

    first = [
        (array, piece, hop)
        for hop in range(1, n_sp)
        for array in range(2)
        for piece in range(splits)
    ]
    second = [(2, piece, hop) for hop in range(1, n_sp) for piece in range(splits)]
    queue = [first + second, 0]

    def advance(count):
        steps, at = queue
        for step in steps[at : at + count]:
            ring_step(*step)
        queue[1] = min(at + count, len(steps))

    unit = max(1, len(first) // 28)

    lat_own.wait()
    for hop in range(1, n_sp + 1):
        for direction in range(2):
            if hop > 1:
                lat_arrival(hop - 1, direction).wait_recv()
                lat_copy(hop - 1, direction).wait_send()
            if hop < n_sp:
                lat_copy(hop, direction).start()
            if hop > 2:
                share_copy(hop - 2, direction, core).wait_send()
            if hop > 1:
                share_copy(hop - 1, direction, core).start()
        if hop < n_sp and queue[1] < 7 * unit:
            advance(1)
    for direction in range(2):
        share_copy(n_sp - 1, direction, core).wait_send()
        for hop in range(1, n_sp):
            share_copy(hop, direction, 1 - core).wait_recv()

    total_rows = n_sp * n_rows
    lat_wide = lat_all.shape[3]
    chunk_blocks = max(1, min(n_sp, 1536 // n_rows))
    chunks = n_sp // chunk_blocks
    chunk = chunk_blocks * n_rows
    half_blocks = max(1, chunk_blocks // 2)

    def project(step):
        rows = half_blocks * n_rows
        lat = lat_all[pl.ds(step * half_blocks, half_blocks)].reshape(rows, lat_wide)
        keys[pl.ds(step * rows, rows)] = dot(lat, wk_ref[...]).astype(jnp.bfloat16)
        values[pl.ds(step * rows, rows)] = dot(lat, wv_ref[...]).astype(jnp.bfloat16)

    if chunks == 1:
        for step in range(n_sp // half_blocks):
            project(step)
            advance(unit)
    else:
        pl.loop(0, n_sp // half_blocks)(project)
        advance(2 * unit)

    score_scale = (NOPE + ROPE) ** (-0.5)
    lane = lax.broadcasted_iota(jnp.int32, (n_rows, LANES), 1)

    def attend(head, at, state):
        maxima, totals, running = state
        rows = pl.ds(at * chunk, chunk)
        columns = slice(head * LANES, (head + 1) * LANES)
        pair = slice(head // 2 * LANES, (head // 2 + 1) * LANES)
        scores = dot_nt(q_ref[head], keys[rows, columns]) * score_scale
        top = jnp.max(scores, axis=1, keepdims=True)
        if maxima is not None:
            top = jnp.maximum(maxima, top)
        probs = jnp.exp(scores - top)
        sums = jnp.sum(probs, axis=1, keepdims=True)
        update = dot(probs.astype(jnp.bfloat16), values[rows, pair])
        if maxima is not None:
            factor = jnp.exp(maxima - top)
            sums = totals * factor + sums
            update = running * factor + update
        return (top, sums, update)

    for head in range(head_count):
        state = attend(head, 0, (None, None, None))
        if chunks > 1:
            state = lax.fori_loop(1, chunks, functools.partial(attend_loop, attend, head), state)
        result = state[2] / state[1]
        pair = slice(head // 2 * LANES, (head // 2 + 1) * LANES)
        if head % 2 == 0:
            heads[:, pair] = result.astype(jnp.bfloat16)
        else:
            heads[:, pair] = jnp.where(
                lane < VDIM, heads[:, pair].astype(jnp.float32), result
            ).astype(jnp.bfloat16)
        advance(unit)

    def tp_copy(stage, slot_source, slot_target, to, slot_semaphore):
        return pltpu.make_async_remote_copy(
            src_ref=slot_source,
            dst_ref=slot_target,
            send_sem=tp_send.at[stage, slot_semaphore],
            recv_sem=tp_recv.at[stage, slot_semaphore],
            device_id={"tp": to},
            device_id_type=MESH,
        )

    def exchange(stage, source_of, target_of):
        copies = []
        for k in range(1, n_tp):
            to = (tp + k) % n_tp
            copies.append(tp_copy(stage, source_of(to), target_of(k), to, k))
        return copies

    copies = exchange(0, lambda to: part_send.at[to], lambda k: part_recv.at[k])
    for k in range(1, n_tp + 1):
        to = (tp + k) % n_tp
        part_send[to] = dot(
            heads[...], wo_ref[:, pl.ds(pl.multiple_of(to * n_cols, LANES), n_cols)]
        ).astype(jnp.bfloat16)
        if k < n_tp:
            copies[k - 1].start()
    advance(4 * unit)
    mixed = DEEP_ALPHA * resid_ref[...].astype(jnp.float32) + part_send[tp].astype(jnp.float32)
    for k in range(1, n_tp):
        copies[k - 1].wait_recv()
        mixed = mixed + part_recv[k].astype(jnp.float32)
    pending = list(copies)

    width_total = n_cols * n_tp

    def normed(rows_in, gain_ref, stage, send, recv, between):
        sums = jnp.sum(rows_in, axis=1, keepdims=True)
        squares = jnp.sum(rows_in * rows_in, axis=1, keepdims=True)
        mine = jnp.where(lane < LANES // 2, sums, squares)
        send[...] = mine
        copies = exchange(stage, lambda to: send, lambda k: recv.at[k])
        for copy in copies:
            copy.start()
        between()
        for k in range(1, n_tp):
            copies[k - 1].wait_recv()
            mine = mine + recv[k]
        pending.extend(copies)
        row_mean = mine[:, :1] / width_total
        variance = mine[:, LANES // 2 : LANES // 2 + 1] / width_total - row_mean * row_mean
        return (
            (rows_in - row_mean) * lax.rsqrt(variance + NORM_EPSILON) * gain_ref[...]
        ).astype(jnp.bfloat16)

    hidden_in = normed(
        mixed, gain_mix_ref, 1, stat_send, stat_recv, lambda: advance(2 * unit)
    )
    rows_all[tp] = hidden_in
    copies = exchange(2, lambda to: rows_all.at[tp], lambda k: rows_all.at[tp])
    for copy in copies:
        copy.start()
    pending.extend(copies)
    advance(4 * unit)
    for k in range(1, n_tp):
        sender = (tp + n_tp - k) % n_tp
        tp_copy(2, rows_all.at[sender], rows_all.at[sender], sender, k).wait_recv()

    advance(len(first) - queue[1])
    advance(splits)

    def last_hop(array):
        for piece in range(splits):
            for direction in range(2):
                ring_copy(array, piece, n_sp - 1, direction, True).wait_recv()
                ring_copy(array, piece, n_sp - 1, direction, False).wait_send()

    last_hop(0)
    group = n_sp // n_tp
    depth = group * wg_ref.shape[0]
    hidden_width = wg_ref.shape[1]

    def wide(weight):
        total = None
        for t in range(n_tp):
            term = dot(
                rows_all[t],
                weight[t * group : (t + 1) * group].reshape(depth, hidden_width),
            )
            total = term if total is None else total + term
        return total

    gate_sum = wide(gate_all)
    advance(splits)
    last_hop(1)
    up_sum = wide(up_all)
    advance(splits)
    hidden = (gate_sum / (1.0 + jnp.exp(-gate_sum)) * up_sum).astype(jnp.bfloat16)

    advance(len(queue[0]))
    last_hop(2)
    copies = exchange(3, lambda to: part2_send.at[to], lambda k: part2_recv.at[k])
    for k in range(1, n_tp + 1):
        to = (tp + k) % n_tp
        part2_send[to] = dot_nt(
            hidden, down_all[pl.ds(to * group, group)].reshape(depth, hidden_width)
        ).astype(jnp.bfloat16)
        if k < n_tp:
            copies[k - 1].start()
    mixer = part2_send[tp].astype(jnp.float32)
    for k in range(1, n_tp):
        copies[k - 1].wait_recv()
        mixer = mixer + part2_recv[k].astype(jnp.float32)
    pending.extend(copies)
    final = DEEP_ALPHA * rows_all[tp].astype(jnp.float32) + HALF_STEP * mixer
    out_ref[...] = normed(final, gain_out_ref, 4, stat2_send, stat2_recv, lambda: None)
    for copy in pending:
        copy.wait_send()


def attend_loop(attend, head, at, state):
    return attend(head, at, state)


def local(
    queries,
    latents,
    rope_key,
    w_key,
    w_value,
    w_out,
    resid,
    gain_mix,
    w_gate,
    w_up,
    w_down,
    gain_out,
):
    n_sp = lax.axis_size("sp")
    n_tp = lax.axis_size("tp")
    rows = queries.shape[0]
    head_count = w_key.shape[1] // NOPE
    rank = latents.shape[1]
    cols = resid.shape[1]
    hidden_width = w_gate.shape[1]
    weight_rows = w_gate.shape[0]
    offset = lax.axis_index("sp") * rows
    positions = offset + jnp.arange(rows, dtype=jnp.int32)
    cosine, sine = rotary_tables(positions, ROPE, GRID_W)
    key_rot = rotate(rope_key, cosine, sine)
    shaped = queries.reshape(rows, head_count, NOPE + ROPE)
    q_rot = rotate(shaped[:, :, NOPE:], cosine[:, None, :], sine[:, None, :])
    spare = LANES - NOPE - ROPE
    q_pad = jnp.concatenate(
        [shaped[:, :, :NOPE], q_rot, jnp.zeros((rows, head_count, spare), jnp.bfloat16)], axis=-1
    )
    q_pad = jnp.transpose(q_pad, (1, 0, 2))
    lat_wide = rank + LANES
    lat_ext = jnp.concatenate(
        [latents, key_rot, jnp.zeros((rows, LANES - ROPE), jnp.bfloat16)], axis=1
    ).reshape(4, rows // 4, lat_wide)
    key_cols = jnp.pad(
        w_key.reshape(rank, head_count, NOPE), ((0, LANES), (0, 0), (0, LANES - NOPE))
    )
    place_rot = jnp.pad(
        jnp.eye(ROPE, dtype=jnp.bfloat16), ((rank, LANES - ROPE), (NOPE, spare))
    )
    key_cols = (key_cols + place_rot[:, None, :]).reshape(lat_wide, head_count * LANES)
    value_cols = jnp.pad(w_value, ((0, LANES), (0, 0)))
    splits = 2 if weight_rows % 64 == 0 else 1
    bf16 = jnp.bfloat16
    total_rows = n_sp * rows
    vmem = pl.BlockSpec(memory_space=pltpu.VMEM)
    anywhere = pl.BlockSpec(memory_space=pl.ANY)
    dma = pltpu.SemaphoreType.DMA
    return pl.pallas_call(
        functools.partial(layer_kernel, n_sp, n_tp, splits),
        out_shape=jax.ShapeDtypeStruct((rows, cols), bf16),
        in_specs=[vmem, anywhere] + [vmem] * 6 + [anywhere] * 3,
        out_specs=vmem,
        scratch_shapes=[
            pltpu.VMEM((n_sp, 4, rows // 4, lat_wide), bf16),
            pltpu.VMEM((total_rows, head_count * LANES), bf16),
            pltpu.VMEM((total_rows, head_count * VDIM), bf16),
            pltpu.VMEM((n_sp, weight_rows, hidden_width), bf16),
            pltpu.VMEM((n_sp, weight_rows, hidden_width), bf16),
            pltpu.VMEM((n_sp, weight_rows, hidden_width), bf16),
            pltpu.VMEM((rows, head_count * VDIM), bf16),
            pltpu.VMEM((n_tp, rows, cols), bf16),
            pltpu.VMEM((n_tp, rows, cols), bf16),
            pltpu.VMEM((rows, LANES), jnp.float32),
            pltpu.VMEM((n_tp, rows, LANES), jnp.float32),
            pltpu.VMEM((n_tp, rows, cols), bf16),
            pltpu.VMEM((n_tp, rows, cols), bf16),
            pltpu.VMEM((n_tp, rows, cols), bf16),
            pltpu.VMEM((rows, LANES), jnp.float32),
            pltpu.VMEM((n_tp, rows, LANES), jnp.float32),
            dma((4,)),
            dma((2,)),
            dma((2, n_sp - 1)),
            dma((2,)),
            dma((2, n_sp - 1)),
            dma((3, splits, 2)),
            dma((3, splits, 2, n_sp - 1)),
            dma((5, n_tp)),
            dma((5, n_tp)),
        ],
        compiler_params=pltpu.CompilerParams(
            collective_id=0, has_side_effects=True, vmem_limit_bytes=66000000
        ),
    )(
        q_pad,
        lat_ext,
        key_cols,
        value_cols,
        w_out,
        resid,
        gain_mix.reshape(1, -1),
        gain_out.reshape(1, -1),
        w_gate,
        w_up,
        w_down.T,
    )


def solution(mesh):
    placed = (
        P("sp", "tp"),
        P("sp", None),
        P("sp", None),
        P(None, "tp"),
        P(None, "tp"),
        P("tp", None),
        P("sp", "tp"),
        P("tp"),
        P("sp", "tp"),
        P("sp", "tp"),
        P("tp", "sp"),
        P("tp"),
    )
    return jax.shard_map(
        local, mesh=mesh, in_specs=placed, out_specs=P("sp", "tp"), check_vma=False
    )
```

time: 325 us -> 137 us (0.42)
  waiting for transfers between devices: 190 us -> 0 us
  Pallas kernels: 0 us -> 126 us
  blocking collectives: 90.5 us -> 0 us
  matrix products: 19.2 us -> 0 us
  between operations: 14.9 us -> 0.15 us
  local copies, waits for them, and re-layouts: 2.7 us -> 6.98 us
  other arithmetic: 6.87 us -> 2.79 us
    all_gather x4 -> x0, waiting for transfers between devices: 144 us -> none  [the longest x1 63.1 us: local(): lax.all_gather(w_down, 'sp', axis=1, tiled=True)]
    pallas_call x0 -> x1, Pallas kernels: none -> 126 us  [local(): pl.pallas_call(functools.partial(layer_kernel, n_sp, n_tp, splits), out_s...]
    all_gather x4 -> x0, blocking collectives: 79 us -> none  [the longest x1 34.8 us: local(): lax.all_gather(latent_part, 'sp', axis=0, tiled=True)]
    reduce_scatter x2 -> x0, waiting for transfers between devices: 44.1 us -> none  [the longest x1 22.5 us: local(): lax.psum_scatter(projected.astype(jnp.bfloat16), 'tp', scatter_dimension=...]
    dot_general x8 -> x0, matrix products: 19.2 us -> none  [the longest x1 5.41 us: local(): jnp.dot(hidden, lax.all_gather(w_down, 'sp', axis=1, tiled=True), preferr...]
    psum x2 -> x0, blocking collectives: 11.5 us -> none  [split_norm(): lax.psum((jnp.sum(rows_in, axis=1), jnp.sum(rows_in * rows_in, axis=1)),...]
  transfers between devices with their start and end apart: 6 -> 0, of which waited for: 5 -> 0; matrix products, arithmetic and copies ran while one was open for 3% -> 0% of each run, Pallas kernels for 0% -> 0%
where the time goes in v1:
time: 137 us; the launch traced here: 136 us
  Pallas kernels  126 us (92%)
  local copies, waits for them, and re-layouts  6.98 us (5%)
  other arithmetic  2.79 us (2%)
    pallas_call x1, Pallas kernels, local(): pl.pallas_call(functools.partial(layer_kernel, n_sp, n_tp, splits), out_s...  126 us
    unnamed x13, local copies, waits for them, and re-layouts  2.84 us

profile of v1, /device:TPU:0, one launch (start us, length us, event | category | flops | bytes accessed | tf_op | source)
XLA Modules:
  0.0 135.9 jit_solution(15166215584764776593)
XLA Ops:
  0.0 0.1 broadcast_multiply_fusion.1
  0.1 0.8 fusion.5
  0.9 1.1 reshape.113
  2.0 0.3 fusion.13
  2.2 0.1 copy.44
  2.4 0.2 copy.34
  2.6 0.2 copy.36
  2.8 0.1 copy.30
  2.9 0.1 copy.33
  3.0 0.1 fusion.1
  3.1 0.0 copy-start.3
  3.1 0.0 copy-start.1
  3.2 0.1 pad.26.clone
  3.2 0.9 maximum_bitcast_fusion.q_ref
  4.1 0.1 copy.37
  4.2 0.1 copy.38
  4.4 0.1 pad.22.clone
  4.4 0.0 copy-done.3
  4.4 0.8 maximum_maximum_fusion
  5.2 0.0 copy-done.1
  5.2 0.1 copy.39
  5.4 0.0 copy-start
  5.4 0.1 pad_add_fusion
  5.5 0.0 copy-start.2
  5.5 1.1 copy.42.wk_ref
  6.6 0.0 copy-done
  6.6 0.9 copy.41
  7.5 0.0 copy-done.2
  7.5 0.8 pad.18.wv_ref
  8.3 126.0 %shard_map.118 = bf16[192,512]{1,0:T(8,128)(2,1)} custom-call(bf16[4,192,128]{2,1,0:T(8,128)(2,1)} %maximum_bitcast_fusion.q_ref, bf16[4,48,640]{2,1,0:T(8,128)(2,1)} %bitcast.13, bf16[640,512]{1,0:T(8,128)(2,1)} %copy.42.wk_ref, bf16[640,256]{1,0:T(8,128)(2,1)} %pad.18.wv_ref, bf16[256,2048]{1,0:T(8,128)(2,1)} %wo_ref.1, bf16[192,512]{1,0:T(8,128)(2,1)} %resid_ref.1, ...), custom_call_target="tpu_custom_call" | custom-call | tf_op jit(solution)/shard_map/pallas_call | solution.py:467
  134.3 1.6 %copy.51 = bf16[192,512]{1,0:T(8,128)(2,1)} copy(bf16[192,512]{1,0:T(8,128)(2,1)} %shard_map.118) | data formatting | bytes 393216
  (8 shorter events, 0.1 us)
Async XLA Ops:
  3.1 1.3 copy-start.3
  3.1 2.1 %copy-start.1 = (bf16[512,256]{1,0:T(8,128)(2,1)S(1)}, bf16[512,256]{1,0:T(8,128)(2,1)}, u32[]{:S(2)}) copy-start(bf16[512,256]{1,0:T(8,128)(2,1)} %param.15) | copy-start | bytes 786436
  5.4 1.2 copy-start
  5.5 2.0 %copy-start.2 = (bf16[512,256]{1,0:T(8,128)(2,1)S(1)}, bf16[512,256]{1,0:T(8,128)(2,1)}, u32[]{:S(2)}) copy-start(bf16[512,256]{1,0:T(8,128)(2,1)} %param.16) | copy-start | bytes 786436

commit v2 on v1

--- a/solution.py
+++ b/solution.py
@@ -20,24 +20,25 @@
 MESH = pl.DeviceIdType.MESH
 
 
-def rotary_tables(positions, rotary_width, grid_width):
-    grid_rows = (positions // grid_width).astype(jnp.float32)
-    grid_cols = (positions % grid_width).astype(jnp.float32)
-    freq_count = rotary_width // 4
-    inverse = ROTARY_BASE ** (-jnp.arange(freq_count, dtype=jnp.float32) / freq_count)
-    angle_table = jnp.concatenate(
-        [grid_rows[:, None] * inverse, grid_cols[:, None] * inverse], axis=-1
-    )
-    return (jnp.cos(angle_table), jnp.sin(angle_table))
+def rotary_tables(first, rows):
+    at = first + lax.broadcasted_iota(jnp.int32, (rows, LANES), 0)
+    column = lax.broadcasted_iota(jnp.int32, (rows, LANES), 1)
+    freq_count = ROPE // 4
+    grid_row = (at // GRID_W).astype(jnp.float32)
+    grid_col = (at % GRID_W).astype(jnp.float32)
+    spot = jnp.where(column % (2 * freq_count) < freq_count, grid_row, grid_col)
+    inverse = jnp.ones((rows, LANES), jnp.float32)
+    for k in range(1, freq_count):
+        inverse = jnp.where(column % freq_count == k, ROTARY_BASE ** (-k / freq_count), inverse)
+    angles = spot * inverse
+    return (jnp.cos(angles)[:, : ROPE // 2], jnp.sin(angles)[:, : ROPE // 2])
 
 
 def rotate(vectors, cosine, sine):
-    half_width = vectors.shape[-1] // 2
-    leading = vectors[..., :half_width].astype(jnp.float32)
-    trailing = vectors[..., half_width:].astype(jnp.float32)
-    return jnp.concatenate(
-        [leading * cosine - trailing * sine, leading * sine + trailing * cosine], axis=-1
-    ).astype(jnp.bfloat16)
+    half_width = ROPE // 2
+    leading = vectors[:, :half_width]
+    trailing = vectors[:, half_width:]
+    return [leading * cosine - trailing * sine, leading * sine + trailing * cosine]
 
 
 def ring_device(place, count):
@@ -64,6 +65,7 @@
     splits,
     q_ref,
     lat_ref,
+    rope_ref,
     wk_ref,
     wv_ref,
     wo_ref,
@@ -76,10 +78,12 @@
     out_ref,
     lat_all,
     keys,
+    rotary,
     values,
     gate_all,
     up_all,
     down_all,
+    q_all,
     heads,
     part_send,
     part_recv,
@@ -90,6 +94,7 @@
     part2_recv,
     stat2_send,
     stat2_recv,
+    hid,
     local_sem,
     lat_send,
     lat_recv,
@@ -99,6 +104,8 @@
     ring_recv,
     tp_send,
     tp_recv,
+    down_send,
+    down_recv,
 ):
     sp = lax.axis_index("sp")
     tp = lax.axis_index("tp")
@@ -108,21 +115,11 @@
     targets = (ahead, behind)
     partner = tp + 1 - 2 * (tp % 2)
     core = tp % 2
-    n_rows = q_ref.shape[1]
-    head_count = q_ref.shape[0]
+    n_rows = q_ref.shape[0]
+    head_count = wk_ref.shape[1] // NOPE
+    rank = wk_ref.shape[0]
     lat_rows = lat_all.shape[2]
     n_cols = out_ref.shape[1]
-
-    own = []
-    lat_own = pltpu.make_async_copy(lat_ref, lat_all.at[sp], local_sem.at[0])
-    lat_own.start()
-    weights = (gate_all, up_all, down_all)
-    for i, (source, target) in enumerate(
-        zip((wg_ref, wu_ref, wd_ref), weights)
-    ):
-        copy = pltpu.make_async_copy(source, target.at[sp], local_sem.at[i + 1])
-        copy.start()
-        own.append(copy)
 
     barrier = pltpu.get_barrier_semaphore()
     for device in targets:
@@ -131,6 +128,44 @@
         pl.semaphore_signal(
             barrier, inc=1, device_id={"tp": (tp + step) % n_tp}, device_id_type=MESH
         )
+
+    own = []
+    lat_own = pltpu.make_async_copy(
+        lat_ref, lat_all.at[sp, :, :, pl.ds(0, rank)], local_sem.at[0]
+    )
+    lat_own.start()
+    weights = (gate_all, up_all, down_all)
+    for i, source in enumerate((wg_ref, wu_ref)):
+        copy = pltpu.make_async_copy(source, weights[i].at[sp], local_sem.at[i + 1])
+        copy.start()
+        own.append(copy)
+    cosine, sine = rotary_tables(sp * n_rows, n_rows)
+    key_rot = rotate(rope_ref[...].astype(jnp.float32), cosine, sine)
+    key_rot.append(jnp.zeros((n_rows, LANES - ROPE), jnp.float32))
+    lat_all[sp, :, :, pl.ds(rank, LANES)] = (
+        jnp.concatenate(key_rot, axis=1).astype(jnp.bfloat16).reshape(4, lat_rows, LANES)
+    )
+
+    def prepare_queries(head):
+        base = head * (NOPE + ROPE)
+        wide_q = q_ref[...].astype(jnp.float32)
+        nope = wide_q[:, base : base + NOPE]
+        other = jnp.zeros((n_rows, NOPE), jnp.float32)
+        rotary = rotate(wide_q[:, base + NOPE : base + NOPE + ROPE], cosine, sine)
+        parts = [nope, other] if head % 2 == 0 else [other, nope]
+        parts = parts + rotary + [jnp.zeros((n_rows, LANES - ROPE), jnp.float32)]
+        q_all[head] = jnp.concatenate(parts, axis=1).astype(jnp.bfloat16)
+
+    def prepare_down():
+        count = wd_ref.shape[1]
+        across = lax.broadcasted_iota(jnp.int32, (count, count), 1)
+        diagonal = (lax.broadcasted_iota(jnp.int32, (count, count), 0) == across).astype(
+            jnp.float32
+        ).astype(jnp.bfloat16)
+        down_all[sp] = dot_nt(diagonal, wd_ref[...]).astype(jnp.bfloat16)
+
+    preparing = [functools.partial(prepare_queries, head) for head in range(head_count)]
+    preparing.append(prepare_down)
     pl.semaphore_wait(barrier, 2 + n_tp - 1)
 
     def origin(hop, direction):
@@ -189,7 +224,7 @@
     started = set()
 
     def ring_step(array, piece, hop):
-        if hop == 1 and array not in started:
+        if hop == 1 and array < 2 and array not in started:
             own[array].wait()
             started.add(array)
         for direction in range(2):
@@ -230,6 +265,10 @@
                 share_copy(hop - 1, direction, core).start()
         if hop < n_sp and queue[1] < 7 * unit:
             advance(1)
+        if preparing:
+            preparing.pop(0)()
+    while preparing:
+        preparing.pop(0)()
     for direction in range(2):
         share_copy(n_sp - 1, direction, core).wait_send()
         for hop in range(1, n_sp):
@@ -244,7 +283,11 @@
 
     def project(step):
         rows = half_blocks * n_rows
-        lat = lat_all[pl.ds(step * half_blocks, half_blocks)].reshape(rows, lat_wide)
+        blocks = pl.ds(step * half_blocks, half_blocks)
+        lat = lat_all[blocks, :, :, pl.ds(0, rank)].reshape(rows, rank)
+        rotary[pl.ds(step * rows, rows)] = lat_all[blocks, :, :, pl.ds(rank, LANES)].reshape(
+            rows, LANES
+        )
         keys[pl.ds(step * rows, rows)] = dot(lat, wk_ref[...]).astype(jnp.bfloat16)
         values[pl.ds(step * rows, rows)] = dot(lat, wv_ref[...]).astype(jnp.bfloat16)
 
@@ -262,9 +305,9 @@
     def attend(head, at, state):
         maxima, totals, running = state
         rows = pl.ds(at * chunk, chunk)
-        columns = slice(head * LANES, (head + 1) * LANES)
         pair = slice(head // 2 * LANES, (head // 2 + 1) * LANES)
-        scores = dot_nt(q_ref[head], keys[rows, columns]) * score_scale
+        whole_keys = jnp.concatenate([keys[rows, pair], rotary[rows]], axis=1)
+        scores = dot_nt(q_all[head], whole_keys) * score_scale
         top = jnp.max(scores, axis=1, keepdims=True)
         if maxima is not None:
             top = jnp.maximum(maxima, top)
@@ -328,7 +371,7 @@
     def normed(rows_in, gain_ref, stage, send, recv, between):
         sums = jnp.sum(rows_in, axis=1, keepdims=True)
         squares = jnp.sum(rows_in * rows_in, axis=1, keepdims=True)
-        mine = jnp.where(lane < LANES // 2, sums, squares)
+        mine = jnp.transpose(jnp.where(lane < 4, sums, squares))[:8]
         send[...] = mine
         copies = exchange(stage, lambda to: send, lambda k: recv.at[k])
         for copy in copies:
@@ -338,8 +381,9 @@
             copies[k - 1].wait_recv()
             mine = mine + recv[k]
         pending.extend(copies)
-        row_mean = mine[:, :1] / width_total
-        variance = mine[:, LANES // 2 : LANES // 2 + 1] / width_total - row_mean * row_mean
+        whole = jnp.transpose(mine) / width_total
+        row_mean = whole[:, :1]
+        variance = whole[:, 4:5] - row_mean * row_mean
         return (
             (rows_in - row_mean) * lax.rsqrt(variance + NORM_EPSILON) * gain_ref[...]
         ).astype(jnp.bfloat16)
@@ -379,34 +423,90 @@
                 weight[t * group : (t + 1) * group].reshape(depth, hidden_width),
             )
             total = term if total is None else total + term
+            advance(1)
         return total
 
     gate_sum = wide(gate_all)
-    advance(splits)
     last_hop(1)
     up_sum = wide(up_all)
-    advance(splits)
     hidden = (gate_sum / (1.0 + jnp.exp(-gate_sum)) * up_sum).astype(jnp.bfloat16)
-
-    advance(len(queue[0]))
-    last_hop(2)
-    copies = exchange(3, lambda to: part2_send.at[to], lambda k: part2_recv.at[k])
-    for k in range(1, n_tp + 1):
-        to = (tp + k) % n_tp
-        part2_send[to] = dot_nt(
-            hidden, down_all[pl.ds(to * group, group)].reshape(depth, hidden_width)
-        ).astype(jnp.bfloat16)
-        if k < n_tp:
-            copies[k - 1].start()
-    mixer = part2_send[tp].astype(jnp.float32)
-    for k in range(1, n_tp):
-        copies[k - 1].wait_recv()
-        mixer = mixer + part2_recv[k].astype(jnp.float32)
-    pending.extend(copies)
+    advance(1)
+
+    half_rows = piece_rows * splits
+    if half_rows % LANES == 0:
+        hid[...] = hidden
+
+        def down_copy(k, slot, to, columns):
+            ref = part2_send.at[to, :, columns]
+            return pltpu.make_async_remote_copy(
+                src_ref=ref,
+                dst_ref=part2_recv.at[k, :, columns],
+                send_sem=down_send.at[k, slot],
+                recv_sem=down_recv.at[k, slot],
+                device_id={"tp": to},
+                device_id_type=MESH,
+            )
+
+        def slot_columns(slot):
+            return pl.ds(pl.multiple_of(slot * half_rows, LANES), half_rows)
+
+        def make_columns(hop):
+            for direction in range(2):
+                block = origin(hop, direction)
+                owner = block // group
+                slot = (block % group) * 2 + direction
+                rows = pl.ds(direction * half_rows, half_rows)
+                part2_send[owner, :, slot_columns(slot)] = dot_nt(
+                    hid[...], down_all[block, rows]
+                ).astype(jnp.bfloat16)
+
+                @pl.when(owner != tp)
+                def send_away():
+                    down_copy((owner + n_tp - tp) % n_tp, slot, owner, slot_columns(slot)).start()
+
+        made = 0
+        while queue[1] < len(queue[0]):
+            array, piece, hop = queue[0][queue[1]]
+            advance(1)
+            if piece == splits - 1:
+                made_to = hop
+                while made < made_to:
+                    make_columns(made)
+                    made += 1
+        while made < n_sp - 1:
+            make_columns(made)
+            made += 1
+        last_hop(2)
+        make_columns(n_sp - 1)
+        mixer = part2_send[tp].astype(jnp.float32)
+        for k in range(1, n_tp):
+            for slot in range(2 * group):
+                down_copy(k, slot, (tp + k) % n_tp, slot_columns(slot)).wait_recv()
+            mixer = mixer + part2_recv[k].astype(jnp.float32)
+    else:
+        advance(len(queue[0]))
+        last_hop(2)
+        copies = exchange(3, lambda to: part2_send.at[to], lambda k: part2_recv.at[k])
+        for k in range(1, n_tp + 1):
+            to = (tp + k) % n_tp
+            part2_send[to] = dot_nt(
+                hidden, down_all[pl.ds(to * group, group)].reshape(depth, hidden_width)
+            ).astype(jnp.bfloat16)
+            if k < n_tp:
+                copies[k - 1].start()
+        mixer = part2_send[tp].astype(jnp.float32)
+        for k in range(1, n_tp):
+            copies[k - 1].wait_recv()
+            mixer = mixer + part2_recv[k].astype(jnp.float32)
+        pending.extend(copies)
     final = DEEP_ALPHA * rows_all[tp].astype(jnp.float32) + HALF_STEP * mixer
     out_ref[...] = normed(final, gain_out_ref, 4, stat2_send, stat2_recv, lambda: None)
     for copy in pending:
         copy.wait_send()
+    if half_rows % LANES == 0:
+        for k in range(1, n_tp):
+            for slot in range(2 * group):
+                down_copy(k, slot, (tp + k) % n_tp, slot_columns(slot)).wait_send()
 
 
 def attend_loop(attend, head, at, state):
@@ -435,29 +535,7 @@
     cols = resid.shape[1]
     hidden_width = w_gate.shape[1]
     weight_rows = w_gate.shape[0]
-    offset = lax.axis_index("sp") * rows
-    positions = offset + jnp.arange(rows, dtype=jnp.int32)
-    cosine, sine = rotary_tables(positions, ROPE, GRID_W)
-    key_rot = rotate(rope_key, cosine, sine)
-    shaped = queries.reshape(rows, head_count, NOPE + ROPE)
-    q_rot = rotate(shaped[:, :, NOPE:], cosine[:, None, :], sine[:, None, :])
-    spare = LANES - NOPE - ROPE
-    q_pad = jnp.concatenate(
-        [shaped[:, :, :NOPE], q_rot, jnp.zeros((rows, head_count, spare), jnp.bfloat16)], axis=-1
-    )
-    q_pad = jnp.transpose(q_pad, (1, 0, 2))
     lat_wide = rank + LANES
-    lat_ext = jnp.concatenate(
-        [latents, key_rot, jnp.zeros((rows, LANES - ROPE), jnp.bfloat16)], axis=1
-    ).reshape(4, rows // 4, lat_wide)
-    key_cols = jnp.pad(
-        w_key.reshape(rank, head_count, NOPE), ((0, LANES), (0, 0), (0, LANES - NOPE))
-    )
-    place_rot = jnp.pad(
-        jnp.eye(ROPE, dtype=jnp.bfloat16), ((rank, LANES - ROPE), (NOPE, spare))
-    )
-    key_cols = (key_cols + place_rot[:, None, :]).reshape(lat_wide, head_count * LANES)
-    value_cols = jnp.pad(w_value, ((0, LANES), (0, 0)))
     splits = 2 if weight_rows % 64 == 0 else 1
     bf16 = jnp.bfloat16
     total_rows = n_sp * rows
@@ -467,25 +545,28 @@
     return pl.pallas_call(
         functools.partial(layer_kernel, n_sp, n_tp, splits),
         out_shape=jax.ShapeDtypeStruct((rows, cols), bf16),
-        in_specs=[vmem, anywhere] + [vmem] * 6 + [anywhere] * 3,
+        in_specs=[vmem, anywhere] + [vmem] * 7 + [anywhere] * 2 + [vmem],
         out_specs=vmem,
         scratch_shapes=[
             pltpu.VMEM((n_sp, 4, rows // 4, lat_wide), bf16),
-            pltpu.VMEM((total_rows, head_count * LANES), bf16),
+            pltpu.VMEM((total_rows, head_count * NOPE), bf16),
+            pltpu.VMEM((total_rows, LANES), bf16),
             pltpu.VMEM((total_rows, head_count * VDIM), bf16),
             pltpu.VMEM((n_sp, weight_rows, hidden_width), bf16),
             pltpu.VMEM((n_sp, weight_rows, hidden_width), bf16),
             pltpu.VMEM((n_sp, weight_rows, hidden_width), bf16),
+            pltpu.VMEM((head_count, rows, 2 * LANES), bf16),
             pltpu.VMEM((rows, head_count * VDIM), bf16),
             pltpu.VMEM((n_tp, rows, cols), bf16),
             pltpu.VMEM((n_tp, rows, cols), bf16),
-            pltpu.VMEM((rows, LANES), jnp.float32),
-            pltpu.VMEM((n_tp, rows, LANES), jnp.float32),
+            pltpu.VMEM((8, rows), jnp.float32),
+            pltpu.VMEM((n_tp, 8, rows), jnp.float32),
             pltpu.VMEM((n_tp, rows, cols), bf16),
             pltpu.VMEM((n_tp, rows, cols), bf16),
             pltpu.VMEM((n_tp, rows, cols), bf16),
-            pltpu.VMEM((rows, LANES), jnp.float32),
-            pltpu.VMEM((n_tp, rows, LANES), jnp.float32),
+            pltpu.VMEM((8, rows), jnp.float32),
+            pltpu.VMEM((n_tp, 8, rows), jnp.float32),
+            pltpu.VMEM((rows, hidden_width), bf16),
             dma((4,)),
             dma((2,)),
             dma((2, n_sp - 1)),
@@ -495,22 +576,25 @@
             dma((3, splits, 2, n_sp - 1)),
             dma((5, n_tp)),
             dma((5, n_tp)),
+            dma((n_tp, 2 * (n_sp // n_tp))),
+            dma((n_tp, 2 * (n_sp // n_tp))),
         ],
         compiler_params=pltpu.CompilerParams(
             collective_id=0, has_side_effects=True, vmem_limit_bytes=66000000
         ),
     )(
-        q_pad,
-        lat_ext,
-        key_cols,
-        value_cols,
+        queries,
+        latents.reshape(4, rows // 4, rank),
+        rope_key,
+        w_key,
+        w_value,
         w_out,
         resid,
         gain_mix.reshape(1, -1),
         gain_out.reshape(1, -1),
         w_gate,
         w_up,
-        w_down.T,
+        w_down,
     )
 
 

time: 137 us -> 123 us (0.90)
  Pallas kernels: 126 us -> 120 us
  local copies, waits for them, and re-layouts: 6.98 us -> 3.05 us
  other arithmetic: 2.79 us -> 0 us
    pallas_call x1, Pallas kernels: 126 us -> 120 us  [local(): pl.pallas_call(functools.partial(layer_kernel, n_sp, n_tp, splits), out_s...]
    reshape x2 -> x0, local copies, waits for them, and re-layouts: 2.15 us -> none  [the longest x1 1.09 us: local(): (key_cols + place_rot[:, None, :]).reshape(lat_wide, head_count * LANES)]
    unnamed x13 -> x2, local copies, waits for them, and re-layouts: 2.84 us -> 3.05 us
where the time goes in v2:
time: 123 us
  Pallas kernels  120 us (98%)
  local copies, waits for them, and re-layouts  3.05 us (2%)
    pallas_call x1, Pallas kernels, local(): pl.pallas_call(functools.partial(layer_kernel, n_sp, n_tp, splits), out_s...  120 us
    unnamed x2, local copies, waits for them, and re-layouts  3.05 us

profile of v2, /device:TPU:0, one launch (start us, length us, event | category | flops | bytes accessed | tf_op | source)
XLA Modules:
  0.0 122.8 jit_solution(12947884380134890903)
XLA Ops:
  0.0 1.4 %copy.13.rope_ref = bf16[192,32]{1,0:T(8,128)(2,1)} copy(bf16[192,32]{0,1:T(8,128)(2,1)} %param.14) | data formatting | bytes 24576 | tf_op args[2]
  1.4 119.7 %shard_map.118 = bf16[192,512]{1,0:T(8,128)(2,1)} custom-call(bf16[192,384]{1,0:T(8,128)(2,1)} %q_ref.1, bf16[4,48,512]{2,1,0:T(8,128)(2,1)} %bitcast.3, bf16[192,32]{1,0:T(8,128)(2,1)} %copy.13.rope_ref, bf16[512,256]{1,0:T(8,128)(2,1)} %wk_ref.1, bf16[512,256]{1,0:T(8,128)(2,1)} %wv_ref.1, bf16[256,2048]{1,0:T(8,128)(2,1)} %wo_ref.1, ...), custom_call_target="tpu_custom_call" | custom-call | tf_op jit(solution)/shard_map/pallas_call | solution.py:545
  121.2 1.6 %copy.15 = bf16[192,512]{1,0:T(8,128)(2,1)} copy(bf16[192,512]{1,0:T(8,128)(2,1)} %shard_map.118) | data formatting | bytes 393216
